TPU v7x, 32 devices: a whole 2x2x4 slice. The times are simulated.
32 devices in a mesh: rep: 2 (over y), fs: 4 (over z), tp: 4 (over x, core).
Axes of the slice: x: 2, y: 2, z: 4, core: 2. Of those that a mesh axis runs over, the one named last changes fastest.
Arguments:
- activations: bfloat16 [2048, 4096], P(None, ('rep', 'fs')), may hold values from -60 to 60
- w_mix_in: bfloat16 [2048, 1024], P('fs', 'tp'), may hold values from -0.125 to 0.125
- w_mix_out: bfloat16 [2048, 1024], P('fs', 'tp'), may hold values from -0.1875 to 0.1875
- w_gate: bfloat16 [2048, 2816], P('fs', 'tp'), may hold values from -0.125 to 0.125
- w_up: bfloat16 [2048, 2816], P('fs', 'tp'), may hold values from -0.125 to 0.125
- w_down: bfloat16 [2048, 2816], P('fs', 'tp'), may hold values from -0.109375 to 0.109375
- pool_scale: float32 [1024], replicated, may hold values from 0.1 to 1.9
- gain_mix: float32 [2048], replicated, may hold values from 0.1 to 1.9
- gain_ffn: float32 [2048], replicated, may hold values from 0.1 to 1.9
- gain_out: float32 [2048], replicated, may hold values from 0.1 to 1.9
Outputs:
- normalized: bfloat16 [2048, 4096], P('tp', ('rep', 'fs'))
All inputs are finite; a program needn't handle non-finite values.
Results may differ from a plain program's by a relative error of at most 0.014.
Values may be sent and summed in bfloat16 or wider, within the bound.
A program may use at most 64 MiB of HBM per device.

v0:
```python
import functools

import jax
import jax.numpy as jnp
from jax import lax
from jax.experimental import pallas as pl
from jax.experimental.pallas import tpu as pltpu
from jax.sharding import PartitionSpec as P

POOL_GROUP = 256
SEQ_LEN = 256
EPS = 1e-06
LANES = 128
MESH = pl.DeviceIdType.MESH
BF = jnp.bfloat16
F32 = jnp.float32


def dot_first(weights, acts):
    return lax.dot_general(weights, acts, (((0,), (0,)), ((), ())), preferred_element_type=F32)


def column(row, width):
    square = jnp.transpose(jnp.broadcast_to(row, (LANES, LANES)))
    return jnp.concatenate([square] * (width // LANES), axis=1)


def body(
    nr, nf, nt,
    act, w_in, w_out, w_gate, w_up, w_down, scale, g_mix, g_ffn, g_out, out,
    b_in, b_out, b_gate, b_up, b_down,
    h, x1, part0, part1, u_acc, pooled, gate_acc, up_acc, hidden, own_x, squares,
    buf_a, buf_b,
    own_sem, zsend, zrecv, ysend, yrecv,
    a_send, a_recv, b_send, b_recv, c_send, c_recv, d_send, d_recv, s_send, s_recv,
):
    r, f, t = lax.axis_index("rep"), lax.axis_index("fs"), lax.axis_index("tp")
    features, tokens = act.shape
    shards = (w_in, w_out, w_gate, w_up, w_down)
    full = (b_in, b_out, b_gate, b_up, b_down)
    rows = w_in.shape[0]
    piece = rows // nr
    share = features // nt
    channels = w_in.shape[1]
    ff = w_gate.shape[1]
    nh = nt // 2
    chip, parity = t // 2, lax.rem(t, 2)
    partner = t + 1 - 2 * parity

    cut = -(-ff // (2 * LANES)) * LANES
    items = [(0, 0, channels), (1, 0, channels)]
    for m in (2, 3, 4):
        items += [(m, 0, cut), (m, cut, ff - cut)]

    own = [pltpu.make_async_copy(shards[m], full[m].at[f], own_sem.at[m]) for m in range(5)]
    for copy in own:
        copy.start()

    barrier = pltpu.get_barrier_semaphore()
    for step in (1, nf - 1):
        pl.semaphore_signal(barrier, inc=1, device_id=(r, lax.rem(f + step, nf), t), device_id_type=MESH)
    for o in range(1, nr):
        pl.semaphore_signal(barrier, inc=1, device_id=(lax.rem(r + o, nr), f, t), device_id_type=MESH)
    for i in range(1, nt):
        pl.semaphore_signal(barrier, inc=1, device_id=(r, f, lax.rem(t + i, nt)), device_id_type=MESH)
    pl.semaphore_wait(barrier, 2 + (nr - 1) + (nt - 1))

    def part_of(m, blk, of):
        matrix, start, size = items[m]
        at = pl.ds(pl.multiple_of(of * piece, piece), piece)
        return full[matrix].at[blk, at, pl.ds(start, size)]

    def z_copy(m, blk, way, d):
        ref = part_of(m, blk, r)
        return pltpu.make_async_remote_copy(
            src_ref=ref, dst_ref=ref,
            send_sem=zsend.at[m, way, lax.rem(d, 2)], recv_sem=zrecv.at[m, blk],
            device_id=(r, f + 1 - 2 * way, t), device_id_type=MESH,
        )

    def y_copy(m, blk, way, d, o):
        ref = part_of(m, blk, r)
        return pltpu.make_async_remote_copy(
            src_ref=ref, dst_ref=ref,
            send_sem=ysend.at[m, way, lax.rem(d, 2), o - 1], recv_sem=yrecv.at[m, blk, o - 1],
            device_id=(lax.rem(r + o, nr), f, t), device_id_type=MESH,
        )

    def y_arrival(m, blk, o):
        source = lax.rem(r - o + nr, nr)
        ref = part_of(m, blk, source)
        return pltpu.make_async_remote_copy(
            src_ref=ref, dst_ref=ref,
            send_sem=ysend.at[m, 0, 0, o - 1], recv_sem=yrecv.at[m, blk, o - 1],
            device_id=(lax.rem(r + o, nr), f, t), device_id_type=MESH,
        )

    can_send = (f + 1 < nf, f >= 1)
    hops = (f, nf - 1 - f)

    def send_own(m):
        if items[m][1] == 0:
            own[items[m][0]].wait()
        for way in (0, 1):
            @pl.when(can_send[way])
            def _():
                z_copy(m, f, way, 0).start()

    def arrival(m, way, d):
        blk = f - d if way == 0 else f + d

        @pl.when(d <= hops[way])
        def _():
            z_copy(m, blk, way, d).wait_recv()

            @pl.when(can_send[way])
            def _():
                @pl.when(d >= 2)
                def _():
                    z_copy(m, blk, way, d).wait_send()

                z_copy(m, blk, way, d).start()

            for o in range(1, nr):
                @pl.when(d >= 3)
                def _():
                    y_copy(m, blk, way, d, o).wait_send()

                y_copy(m, blk, way, d, o).start()

    def gather(m, low, high):
        if low >= high:
            return

        def rounds(d, carry):
            arrival(m, 0, d)
            arrival(m, 1, d)
            return carry

        if low == 1:
            rounds(jnp.int32(1), 0)
            if m + 1 < len(items):
                send_own(m + 1)
            low = 2
        lax.fori_loop(low, high, rounds, 0)

    def finish(m):
        def one(blk, carry):
            @pl.when(blk != f)
            def _():
                for o in range(1, nr):
                    y_arrival(m, blk, o).wait_recv()
            return carry

        lax.fori_loop(0, nf, one, 0)

    def drain(m):
        for way in (0, 1):
            for back in (0, 1):
                last = hops[way] - back

                @pl.when(jnp.logical_and(can_send[way], last >= 0))
                def _():
                    z_copy(m, f, way, last).wait_send()

                @pl.when(last >= 1)
                def _():
                    for o in range(1, nr):
                        y_copy(m, f, way, last, o).wait_send()

    def share_of(ref, j):
        return ref.at[pl.ds(pl.multiple_of(j * share, share), share), :]

    def normalize(load, gain, store, count):
        def square(i, total):
            v = load(i)
            return total + jnp.sum(v * v, axis=0, keepdims=True)

        total = lax.fori_loop(0, count, square, jnp.zeros((1, tokens), F32))
        factor = lax.rsqrt(total / features + EPS)

        def scaled(i, carry):
            store(i, load(i) * factor * column(gain[pl.ds(i, 1), :], tokens))
            return carry

        lax.fori_loop(0, count, scaled, 0)

    def chunk(ref, i):
        return ref[pl.ds(pl.multiple_of(i * LANES, LANES), LANES), :].astype(F32)

    def put(ref):
        def store(i, v):
            ref[pl.ds(pl.multiple_of(i * LANES, LANES), LANES), :] = v.astype(ref.dtype)
        return store

    def a_copy(k, part, c):
        return pltpu.make_async_remote_copy(
            src_ref=share_of(part, 2 * c + 1 - parity), dst_ref=buf_a.at[k, c],
            send_sem=a_send.at[k, c], recv_sem=a_recv.at[k, c],
            device_id=(r, f, partner), device_id_type=MESH,
        )

    def b_copy(k, part, i):
        target = 2 * lax.rem(chip + i, nh) + parity
        return pltpu.make_async_remote_copy(
            src_ref=share_of(part, target), dst_ref=buf_b.at[k, i],
            send_sem=b_send.at[k, i], recv_sem=b_recv.at[k, i],
            device_id=(r, f, target), device_id_type=MESH,
        )

    def start_pair(k, part):
        for i in range(nh):
            a_copy(k, part, i).start()

    def start_chips(k, part):
        for i in range(1, nh):
            c = lax.rem(chip + i, nh)
            target = 2 * c + parity
            a_copy(k, part, c).wait()

            def add(n, carry):
                at = pl.ds(pl.multiple_of(target * share + n * LANES, LANES), LANES)
                mine = part[at, :].astype(F32)
                theirs = buf_a[k, c, pl.ds(pl.multiple_of(n * LANES, LANES), LANES), :].astype(F32)
                part[at, :] = (mine + theirs).astype(BF)
                return carry

            lax.fori_loop(0, share // LANES, add, 0)
            b_copy(k, part, i).start()

    def finish_chips(k, part, base, store):
        a_copy(k, part, chip).wait()
        for i in range(1, nh):
            b_copy(k, part, i).wait()

        def add(n, carry):
            here = pl.ds(pl.multiple_of(n * LANES, LANES), LANES)
            at = pl.ds(pl.multiple_of(t * share + n * LANES, LANES), LANES)
            total = part[at, :].astype(F32) + buf_a[k, chip, here, :].astype(F32)
            for i in range(1, nh):
                total = total + buf_b[k, i, here, :].astype(F32)
            store(n, base[at, :].astype(F32) + total)
            return carry

        lax.fori_loop(0, share // LANES, add, 0)

    def c_copy(i):
        ref = share_of(x1, t)
        return pltpu.make_async_remote_copy(
            src_ref=ref, dst_ref=ref, send_sem=c_send.at[i], recv_sem=c_recv.at[i],
            device_id=(r, f, 2 * lax.rem(chip + i, nh) + parity), device_id_type=MESH,
        )

    def d_copy(i):
        ref = share_of(x1, 2 * lax.rem(chip - i + nh, nh) + parity)
        return pltpu.make_async_remote_copy(
            src_ref=ref, dst_ref=ref, send_sem=d_send.at[i], recv_sem=d_recv.at[i],
            device_id=(r, f, partner), device_id_type=MESH,
        )

    def s_copy(i):
        return pltpu.make_async_remote_copy(
            src_ref=squares.at[0], dst_ref=squares.at[i], send_sem=s_send.at[i], recv_sem=s_recv.at[i],
            device_id=(r, f, lax.rem(t + i, nt)), device_id_type=MESH,
        )

    send_own(0)
    normalize(functools.partial(chunk, act), g_mix, put(h), features // LANES)

    gather(0, 1, nf)
    gather(1, 1, nf)
    finish(0)
    u_acc[...] = jnp.zeros_like(u_acc)

    def mix_in(b, carry):
        at = pl.ds(pl.multiple_of(b * rows, rows), rows)
        u_acc[...] += dot_first(b_in[b], h[at, :])
        return carry

    lax.fori_loop(0, nf, mix_in, 0)
    for i in range(channels // LANES):
        first = t * channels + i * LANES
        window = jnp.int32(2) << (first // POOL_GROUP)
        behind = window // 2
        onward = window - behind
        source = lax.broadcasted_iota(jnp.int32, (SEQ_LEN, SEQ_LEN), 0)
        place = lax.broadcasted_iota(jnp.int32, (SEQ_LEN, SEQ_LEN), 1)
        inside = jnp.logical_and(source >= place - behind, source < place + onward)
        band = jnp.where(inside, 1.0, 0.0).astype(BF)
        spot = lax.broadcasted_iota(jnp.int32, (1, SEQ_LEN), 1)
        count = (jnp.minimum(spot + onward, SEQ_LEN) - jnp.maximum(spot - behind, 0)).astype(F32)
        gain = column(scale[pl.ds(first // LANES, 1), :], SEQ_LEN)
        for s in range(tokens // SEQ_LEN):
            at = (pl.ds(i * LANES, LANES), pl.ds(s * SEQ_LEN, SEQ_LEN))
            u = u_acc[at].astype(BF)
            mean = jnp.dot(u, band, preferred_element_type=F32) / count
            pooled[at] = ((mean - u.astype(F32)) * gain).astype(BF)

    gather(2, 1, nf)
    finish(1)

    def mix_out(b, carry):
        at = pl.ds(pl.multiple_of(b * rows, rows), rows)
        part0[at, :] = jnp.dot(b_out[b], pooled[...], preferred_element_type=F32).astype(BF)
        return carry

    lax.fori_loop(0, nf, mix_out, 0)
    start_pair(0, part0)
    gather(3, 1, nf)
    start_chips(0, part0)
    gather(4, 1, nf)

    def keep_x1(n, v):
        at = pl.ds(pl.multiple_of(t * share + n * LANES, LANES), LANES)
        x1[at, :] = v.astype(BF)

    finish_chips(0, part0, act, keep_x1)
    for i in range(1, nh):
        c_copy(i).start()
    d_copy(0).start()
    gather(5, 1, nf)
    for i in range(1, nh):
        c_copy(i).wait()
        d_copy(i).start()
    gather(6, 1, nf)
    for i in range(nh):
        d_copy(i).wait()
    normalize(functools.partial(chunk, x1), g_ffn, put(h), features // LANES)
    finish(2)
    finish(3)
    gate_acc[...] = jnp.zeros_like(gate_acc)
    up_acc[...] = jnp.zeros_like(up_acc)

    def project(source, acc):
        def one(b, carry):
            at = pl.ds(pl.multiple_of(b * rows, rows), rows)
            acc[...] += dot_first(source[b], h[at, :])
            return carry

        lax.fori_loop(0, nf, one, 0)

    gather(7, 1, nf)
    project(b_gate, gate_acc)
    finish(4)
    finish(5)
    project(b_up, up_acc)
    step = 32

    def activate(n, carry):
        at = pl.ds(pl.multiple_of(n * step, step), step)
        v = gate_acc[at, :]
        hidden[at, :] = (v / (1.0 + jnp.exp(-v)) * up_acc[at, :]).astype(BF)
        return carry

    lax.fori_loop(0, ff // step, activate, 0)
    finish(6)
    finish(7)

    def mlp_out(b, carry):
        at = pl.ds(pl.multiple_of(b * rows, rows), rows)
        part1[at, :] = jnp.dot(b_down[b], hidden[...], preferred_element_type=F32).astype(BF)
        return carry

    if share % rows == 0:
        blocks = share // rows

        def pair_out(c):
            theirs, ours = 2 * c + 1 - parity, 2 * c + parity
            lax.fori_loop(theirs * blocks, (theirs + 1) * blocks, mlp_out, 0)
            a_copy(1, part1, c).start()
            lax.fori_loop(ours * blocks, (ours + 1) * blocks, mlp_out, 0)

        for i in range(1, nh):
            pair_out(lax.rem(chip + i, nh))
        start_chips(1, part1)
        pair_out(chip)
    else:
        lax.fori_loop(0, nf, mlp_out, 0)
        start_pair(1, part1)
        start_chips(1, part1)
    for m in range(len(items)):
        drain(m)
    finish_chips(1, part1, x1, put(own_x))

    def square(i, total):
        v = chunk(own_x, i)
        return total + jnp.sum(v * v, axis=0, keepdims=True)

    mine = lax.fori_loop(0, share // LANES, square, jnp.zeros((1, tokens), F32))
    squares[0] = jnp.broadcast_to(mine, squares.shape[1:])
    for i in range(1, nt):
        s_copy(i).start()
    for i in range(1, nt):
        s_copy(i).wait()
    total = squares[0, pl.ds(0, 1), :]
    for i in range(1, nt):
        total = total + squares[i, pl.ds(0, 1), :]
    factor = lax.rsqrt(total / features + EPS)

    def closing(i, carry):
        gain = column(g_out[pl.ds(t * (share // LANES) + i, 1), :], tokens)
        put(out)(i, chunk(own_x, i) * factor * gain)
        return carry

    lax.fori_loop(0, share // LANES, closing, 0)


def solution(mesh):
    nr, nf, nt = mesh.shape["rep"], mesh.shape["fs"], mesh.shape["tp"]

    def on_device(act, w_in, w_out, w_gate, w_up, w_down, scale, g_mix, g_ffn, g_out):
        features, tokens = act.shape
        rows, channels = w_in.shape
        ff = w_gate.shape[1]
        share = features // nt
        nh = nt // 2
        anywhere = pl.BlockSpec(memory_space=pl.ANY)
        vmem = pl.BlockSpec(memory_space=pltpu.VMEM)
        dma = pltpu.SemaphoreType.DMA
        scratch = [
            pltpu.VMEM((nf, rows, channels), BF),
            pltpu.VMEM((nf, rows, channels), BF),
            pltpu.VMEM((nf, rows, ff), BF),
            pltpu.VMEM((nf, rows, ff), BF),
            pltpu.VMEM((nf, rows, ff), BF),
            pltpu.VMEM((features, tokens), BF),
            pltpu.VMEM((features, tokens), BF),
            pltpu.VMEM((features, tokens), BF),
            pltpu.VMEM((features, tokens), BF),
            pltpu.VMEM((channels, tokens), F32),
            pltpu.VMEM((channels, tokens), BF),
            pltpu.VMEM((ff, tokens), F32),
            pltpu.VMEM((ff, tokens), F32),
            pltpu.VMEM((ff, tokens), BF),
            pltpu.VMEM((share, tokens), F32),
            pltpu.VMEM((nt, 8, tokens), F32),
            pltpu.VMEM((2, nh, share, tokens), BF),
            pltpu.VMEM((2, nh, share, tokens), BF),
            dma((5,)),
            dma((8, 2, 2)),
            dma((8, nf)),
            dma((8, 2, 2, max(nr - 1, 1))),
            dma((8, nf, max(nr - 1, 1))),
            dma((2, nh)), dma((2, nh)), dma((2, nh)), dma((2, nh)),
            dma((nh,)), dma((nh,)), dma((nh,)), dma((nh,)),
            dma((nt,)), dma((nt,)),
        ]
        return pl.pallas_call(
            functools.partial(body, nr, nf, nt),
            out_shape=jax.ShapeDtypeStruct((share, tokens), BF),
            in_specs=[vmem] + [anywhere] * 5 + [vmem] * 4,
            out_specs=vmem,
            scratch_shapes=scratch,
            compiler_params=pltpu.CompilerParams(
                collective_id=0, has_side_effects=True, vmem_limit_bytes=60 * 1024 * 1024
            ),
        )(
            act, w_in, w_out, w_gate, w_up, w_down,
            *[v.reshape(-1, LANES) for v in (scale, g_mix, g_ffn, g_out)],
        )

    weight = P("fs", "tp")
    tokens_split = P(None, ("rep", "fs"))
    return jax.shard_map(
        on_device,
        mesh=mesh,
        in_specs=(tokens_split, *[weight] * 5, P(), P(), P(), P()),
        out_specs=P("tp", ("rep", "fs")),
        check_vma=False,
    )
```

profile of v0, /device:TPU:0, one launch (start us, length us, event | category | flops | bytes accessed | tf_op | source)
XLA Modules:
  0.0 140.6 jit_solution(14266252826345036438)
XLA Ops:
  0.0 0.0 copy-start
  0.0 2.3 %copy.11.w_gate = bf16[512,704]{1,0:T(8,128)(2,1)} copy(bf16[512,704]{0,1:T(8,128)(2,1)} %param.13) | data formatting | bytes 1441792 | tf_op args[3]
  2.3 2.3 %copy.12.w_up = bf16[512,704]{1,0:T(8,128)(2,1)} copy(bf16[512,704]{0,1:T(8,128)(2,1)} %param.14) | data formatting | bytes 1441792 | tf_op args[4]
  4.6 0.0 copy-done
  4.6 1.2 copy.13.w_down
  5.8 132.9 %shard_map.100 = bf16[512,512]{1,0:T(8,128)(2,1)} custom-call(bf16[2048,512]{1,0:T(8,128)(2,1)} %act.1, bf16[512,256]{1,0:T(8,128)(2,1)} %w_in.1, bf16[512,256]{1,0:T(8,128)(2,1)} %w_out.1, bf16[512,704]{1,0:T(8,128)(2,1)} %copy.11.w_gate, bf16[512,704]{1,0:T(8,128)(2,1)} %copy.12.w_up, bf16[512,704]{1,0:T(8,128)(2,1)} %copy.13.w_down, f32[8,128]{1,0:T(8,128)} %bitcast.7, ...), custom_call_target="tpu_custom_call" | custom-call | tf_op jit(solution)/shard_map/pallas_call | solution.py:448
  138.8 1.9 %copy.15 = bf16[512,512]{1,0:T(8,128)(2,1)} copy(bf16[512,512]{1,0:T(8,128)(2,1)} %shard_map.100) | data formatting | bytes 1048576
Async XLA Ops:
  0.0 4.6 %copy-start = (bf16[512,704]{0,1:T(8,128)(2,1)S(1)}, bf16[512,704]{0,1:T(8,128)(2,1)}, u32[]{:S(2)}) copy-start(bf16[512,704]{0,1:T(8,128)(2,1)} %param.15) | copy-start | bytes 2162692
where the time goes:
time: 141 us
  Pallas kernels  133 us (94%)
  local copies, waits for them, and re-layouts  7.67 us (5%)
    pallas_call x1, Pallas kernels, on_device(): pl.pallas_call(functools.partial(body, nr, nf, nt), out_shape=jax.ShapeDt...  133 us
    unnamed x6, local copies, waits for them, and re-layouts  7.67 us

commit v1 on v0

--- a/solution.py
+++ b/solution.py
@@ -405,8 +405,706 @@
     lax.fori_loop(0, share // LANES, closing, 0)
 
 
+def staged(
+    nr, nf, nt,
+    act, w_in, w_out, w_gate, w_up, w_down, scale, g_mix, g_ffn, g_out, out,
+    b_in, b_out, b_gate, b_up, b_down,
+    x0, h, x1, part, pooled, gate_acc, up_acc, hidden, own_x, squares,
+    buf_a, buf_b, back, home,
+    own_sem, act_sem, in_send, out_send, zrecv, wsend, wrecv, ysend, yrecv, v_send, v_recv,
+    a_send, a_recv, b_send, b_recv, c_send, c_recv, d_send, d_recv,
+    e_send, e_recv, g_send, g_recv, s_send, s_recv,
+):
+    r, f, t = lax.axis_index("rep"), lax.axis_index("fs"), lax.axis_index("tp")
+    features, tokens = act.shape
+    shards = (w_in, w_out, w_gate, w_up, w_down)
+    full = (b_in, b_out, b_gate, b_up, b_down)
+    rows, channels = w_in.shape
+    ff = w_gate.shape[0]
+    share = features // nt
+    nh = nt // 2
+    nq = share // LANES
+    chip, parity = t // 2, lax.rem(t, 2)
+    partner = t + 1 - 2 * parity
+    other_rep = lax.rem(r + 1, nr)
+    cuts = 2
+    slab = share // cuts
+    items = [(0, 0), (0, 1), (1, 0), (1, 1), (2, 0), (3, 0), (2, 1), (3, 1), (4, 0), (4, 1)]
+    early = 4
+    extra = 7
+    last = len(items)
+    left = f < nf // 2
+    inner = jnp.logical_and(f >= 1, f < nf - 1)
+    outer = jnp.logical_not(inner)
+    mate = jnp.where(left, 1 - f, 2 * nf - 3 - f)
+    inward = jnp.where(left, f + 1, f - 1)
+    over = jnp.where(inner, nf - 1 - f, nf - 1 - mate)
+    far = jnp.where(inner, nf - 1 - mate, nf - 1 - f)
+    blocks = (mate, over, far)
+
+    own = [pltpu.make_async_copy(shards[m], full[m].at[f], own_sem.at[m]) for m in range(5)]
+    quarter = features // 4
+    stream = [
+        pltpu.make_async_copy(act.at[pl.ds(i * quarter, quarter)], x0.at[pl.ds(i * quarter, quarter)], act_sem.at[i])
+        for i in range(4)
+    ]
+    own[0].start()
+    own[1].start()
+    for copy in stream:
+        copy.start()
+    for copy in own[2:]:
+        copy.start()
+
+    barrier = pltpu.get_barrier_semaphore()
+    for step in (1, nf - 1):
+        pl.semaphore_signal(barrier, inc=1, device_id=(r, lax.rem(f + step, nf), t), device_id_type=MESH)
+    pl.semaphore_signal(barrier, inc=1, device_id=(other_rep, f, t), device_id_type=MESH)
+    for i in range(1, nt):
+        pl.semaphore_signal(barrier, inc=1, device_id=(r, f, lax.rem(t + i, nt)), device_id_type=MESH)
+    pl.semaphore_wait(barrier, 3 + (nt - 1))
+
+    def line(start, size=LANES):
+        return pl.ds(pl.multiple_of(start, size), size)
+
+    def part_of(m, blk, of):
+        matrix, s = items[m]
+        if matrix < 2:
+            size = rows // cuts // nr
+            return full[matrix].at[blk, line((s * nr + of) * size, size), :]
+        if matrix < 4:
+            size = ff // cuts // nr
+            return full[matrix].at[blk, line((s * nr + of) * size, size), :]
+        size = rows // cuts // nr
+        return full[matrix].at[blk, :, line((s * nr + of) * size, size)]
+
+    def remote(ref, dst, send, recv, device):
+        return pltpu.make_async_remote_copy(
+            src_ref=ref, dst_ref=dst, send_sem=send, recv_sem=recv, device_id=device, device_id_type=MESH
+        )
+
+    def in_copy(m, blk, d):
+        ref = part_of(m, blk, r)
+        return remote(ref, ref, in_send.at[m, d], zrecv.at[m, blk], (r, inward, t))
+
+    def out_copy(m, blk, d):
+        ref = part_of(m, blk, r)
+        return remote(ref, ref, out_send.at[m, d], zrecv.at[m, blk], (r, mate, t))
+
+    def w_copy(m, blk):
+        ref = part_of(m, blk, other_rep)
+        return remote(ref, ref, wsend.at[m], wrecv.at[m], (r, mate, t))
+
+    def v_copy(blk):
+        ref = part_of(extra, blk, other_rep)
+        return remote(ref, ref, v_send.at[0], v_recv.at[0], (r, inward, t))
+
+    def y_copy(m, blk, of):
+        ref = part_of(m, blk, of)
+        return remote(ref, ref, ysend.at[m, blk], yrecv.at[m, blk], (other_rep, f, t))
+
+    def own_ready(m):
+        if items[m][1] == 0:
+            own[items[m][0]].wait()
+
+    def send_mixer(m):
+        own_ready(m)
+        in_copy(m, f, 0).start()
+
+        @pl.when(inner)
+        def _():
+            out_copy(m, f, 0).start()
+
+    def hop(m, j):
+        blk = blocks[j]
+        in_copy(m, blk, 0).wait_recv()
+        if j == 0:
+            in_copy(m, blk, 1).start()
+        else:
+            out_copy(m, blk, j).start()
+
+    def side(m, j):
+        y_copy(m, blocks[j], r).start()
+
+    def relay(m, j):
+        hop(m, j)
+        side(m, j)
+
+    def collect(m, j):
+        in_copy(m, blocks[j], 0).wait_recv()
+        y_copy(m, blocks[j], r).start()
+
+    def y_arrival(m, blk):
+        y_copy(m, blk, other_rep).wait_recv()
+
+    def finish(m):
+        for blk in blocks:
+            y_arrival(m, blk)
+
+    def send_inner(m):
+        in_copy(m, f, 0).start()
+
+    def send_outer(m):
+        in_copy(m, f, 0).start()
+        w_copy(m, f).start()
+
+    def pass_on(m):
+        if m < last:
+            in_copy(m, mate, 0).wait_recv()
+            in_copy(m, mate, 1).start()
+
+    def cross(m, *some):
+        for blk in some:
+            in_copy(m, blk, 0).wait_recv()
+            if m != extra or blk is far:
+                y_copy(m, blk, r).start()
+
+    def settle(m):
+        w_copy(m, mate).wait_recv()
+        if m == extra:
+            v_copy(over).wait_recv()
+        else:
+            y_arrival(m, over)
+        y_arrival(m, far)
+
+    def spot(target, q, size=LANES):
+        return line(target * share + q * size, size)
+
+    def normalize(load, gain, store, count):
+        def square(i, total):
+            v = load(i)
+            return total + jnp.sum(v * v, axis=0, keepdims=True)
+
+        total = lax.fori_loop(0, count, square, jnp.zeros((1, tokens), F32))
+        factor = lax.rsqrt(total / features + EPS)
+
+        def scaled(i, carry):
+            store(i, load(i) * factor * column(gain[pl.ds(i, 1), :], tokens))
+            return carry
+
+        lax.fori_loop(0, count, scaled, 0)
+
+    def chunk(ref, i):
+        return ref[line(i * LANES), :].astype(F32)
+
+    def put(ref):
+        def store(i, v):
+            ref[line(i * LANES), :] = v.astype(ref.dtype)
+        return store
+
+    def a_copy(k, target, q, size):
+        return remote(
+            part.at[k, spot(target, q, size)], buf_a.at[k, target // 2, line(q * size, size)],
+            a_send.at[k, target // 2, q], a_recv.at[k, target // 2, q], (r, f, partner),
+        )
+
+    def b_copy(k, i, q, size):
+        target = 2 * lax.rem(chip + i, nh) + parity
+        return remote(
+            part.at[k, spot(target, q, size)], buf_b.at[k, i, line(q * size, size)],
+            b_send.at[k, i, q], b_recv.at[k, i, q], (r, f, target),
+        )
+
+    def c_copy(k, i, q):
+        ref = x1.at[k, spot(t, q)]
+        device = (r, f, 2 * lax.rem(chip + i, nh) + parity)
+        return remote(ref, ref, c_send.at[k, i, q], c_recv.at[k, i, q], device)
+
+    def d_copy(k, i, q):
+        ref = x1.at[k, spot(2 * lax.rem(chip - i + nh, nh) + parity, q)]
+        return remote(ref, ref, d_send.at[k, i, q], d_recv.at[k, i, q], (r, f, partner))
+
+    def e_copy(q):
+        return remote(x1.at[0, spot(t, q)], x1.at[1, spot(t, q)], e_send.at[q], e_recv.at[q], (r, mate, t))
+
+    def g_copy(q):
+        return remote(back.at[line(q * LANES)], home.at[line(q * LANES)], g_send.at[q], g_recv.at[q], (r, mate, t))
+
+    def s_copy(i):
+        return remote(squares.at[0], squares.at[i], s_send.at[i], s_recv.at[i], (r, f, lax.rem(t + i, nt)))
+
+    def add_pair(k, target, q, size):
+        for n in range(size // LANES):
+            here = line(q * size + n * LANES)
+            at = line(target * share + q * size + n * LANES)
+            mine, theirs = part[k, at, :].astype(F32), buf_a[k, target // 2, here, :].astype(F32)
+            part[k, at, :] = (mine + theirs).astype(BF)
+
+    def total_of(k, q):
+        here = line(q * LANES)
+        total = part[k, spot(t, q), :].astype(F32) + buf_a[k, chip, here, :].astype(F32)
+        for i in range(1, nh):
+            total = total + buf_b[k, i, here, :].astype(F32)
+        return total
+
+    send_mixer(0)
+    send_mixer(1)
+    for m in (2, 4, 5, 8):
+        own_ready(m)
+
+    @pl.when(outer)
+    def _():
+        for m in (2, 3):
+            in_copy(m, f, 0).start()
+        for m in (4, 5, 6):
+            send_outer(m)
+        in_copy(7, f, 0).start()
+
+    @pl.when(inner)
+    def _():
+        in_copy(2, f, 0).start()
+
+    for copy in stream:
+        copy.wait()
+    normalize(functools.partial(chunk, x0), g_mix, put(h.at[0]), features // LANES)
+
+    @pl.when(inner)
+    def _():
+        relay(0, 0)
+        relay(0, 1)
+        relay(1, 0)
+        relay(1, 1)
+        in_copy(3, f, 0).start()
+        hop(2, 0)
+        hop(3, 0)
+        send_inner(4)
+        for m in (2, 3):
+            out_copy(m, f, 0).start()
+        relay(0, 2)
+        relay(1, 2)
+        side(2, 0)
+        side(3, 0)
+        relay(2, 1)
+        relay(3, 1)
+        pass_on(4)
+        send_inner(5)
+
+    @pl.when(outer)
+    def _():
+        for j in range(3):
+            collect(0, j)
+            collect(1, j)
+
+    finish(0)
+    finish(1)
+
+    u_mix = dot_first(b_in[0], h[0, pl.ds(0, rows), :])
+    for b in range(1, nf):
+        u_mix += dot_first(b_in[b], h[0, pl.ds(b * rows, rows), :])
+    gate_acc[pl.ds(0, channels), :] = u_mix
+    for i in range(channels // LANES):
+        first = t * channels + i * LANES
+        window = jnp.int32(2) << (first // POOL_GROUP)
+        behind = window // 2
+        onward = window - behind
+        source = lax.broadcasted_iota(jnp.int32, (SEQ_LEN, SEQ_LEN), 0)
+        place = lax.broadcasted_iota(jnp.int32, (SEQ_LEN, SEQ_LEN), 1)
+        inside = jnp.logical_and(source >= place - behind, source < place + onward)
+        band = jnp.where(inside, 1.0, 0.0).astype(BF)
+        seat = lax.broadcasted_iota(jnp.int32, (1, SEQ_LEN), 1)
+        count = (jnp.minimum(seat + onward, SEQ_LEN) - jnp.maximum(seat - behind, 0)).astype(F32)
+        gain = column(scale[pl.ds(first // LANES, 1), :], SEQ_LEN)
+        for s in range(tokens // SEQ_LEN):
+            at = (pl.ds(i * LANES, LANES), pl.ds(s * SEQ_LEN, SEQ_LEN))
+            u = gate_acc[at].astype(BF)
+            mean = jnp.dot(u, band, preferred_element_type=F32) / count
+            pooled[at] = ((mean - u.astype(F32)) * gain).astype(BF)
+
+    mixed = True
+
+    @pl.when(inner)
+    def _():
+        relay(2, 2)
+        relay(3, 2)
+        cross(4, over)
+        pass_on(5)
+        send_inner(6)
+        cross(4, far)
+
+    @pl.when(outer)
+    def _():
+        for j in range(3):
+            collect(2, j)
+            collect(3, j)
+
+    finish(2)
+    finish(3)
+
+    def mix_out(target):
+        part[0, line(target * share, share), :] = jnp.dot(
+            b_out[target], pooled[...], preferred_element_type=F32
+        ).astype(BF)
+
+    for i in range(1, nh + 1):
+        c = lax.rem(chip + i, nh)
+        mix_out(2 * c + 1 - parity)
+        a_copy(0, 2 * c + 1 - parity, 0, share).start()
+        mix_out(2 * c + parity)
+    for i in range(1, nh):
+        target = 2 * lax.rem(chip + i, nh) + parity
+        a_copy(0, target, 0, share).wait_recv()
+        for q in range(nq):
+            add_pair(0, target, q, LANES)
+            b_copy(0, i, q, LANES).start()
+    a_copy(0, t, 0, share).wait_recv()
+
+    @pl.when(inner)
+    def _():
+        cross(5, over)
+
+    for q in range(nq):
+        for i in range(1, nh):
+            b_copy(0, i, q, LANES).wait_recv()
+        x1[0, spot(t, q), :] = (x0[spot(t, q), :].astype(F32) + total_of(0, q)).astype(BF)
+
+        @pl.when(inner)
+        def _():
+            for i in range(1, nh):
+                c_copy(0, i, q).start()
+            d_copy(0, 0, q).start()
+            if q == 0:
+                pass_on(6)
+                send_inner(7)
+                cross(5, far)
+            if q == 1:
+                cross(6, over)
+            if q == 2:
+                pass_on(7)
+                send_inner(8)
+                v_copy(f).start()
+
+        @pl.when(outer)
+        def _():
+            e_copy(q).start()
+            if q == 0:
+                w_copy(7, f).start()
+            if q == 1:
+                in_copy(8, f, 0).start()
+            if q == 3:
+                in_copy(9, f, 0).start()
+
+    cut = ff // cuts
+    step = 32
+    wide = 2 * LANES
+
+    def project(k, s):
+        at = pl.ds(s * cut, cut)
+        for source, acc in ((b_gate, gate_acc), (b_up, up_acc)):
+            def tokens_at(n, carry):
+                here = line(n * wide, wide)
+                total = jnp.dot(source[0, at, :], h[k, pl.ds(0, rows), here], preferred_element_type=F32)
+                for b in range(1, nf):
+                    total += jnp.dot(source[b, at, :], h[k, pl.ds(b * rows, rows), here], preferred_element_type=F32)
+                acc[at, here] = total
+                return carry
+
+            lax.fori_loop(0, tokens // wide, tokens_at, 0)
+
+        def activate(n, carry):
+            here = line(s * cut + n * step, step)
+            v = gate_acc[here, :]
+            hidden[k, here, :] = (v / (1.0 + jnp.exp(-v)) * up_acc[here, :]).astype(BF)
+            return carry
+
+        lax.fori_loop(0, cut // step, activate, 0)
+
+    def mlp_out(k, target, s):
+        at = spot(target, s, slab)
+        part[1 + k, at, :] = dot_first(b_down[target, :, line(s * slab, slab)], hidden[k]).astype(BF)
+
+        @pl.when(lax.rem(target, 2) != parity)
+        def _():
+            a_copy(1 + k, target, s, slab).start()
+
+    def pair_up(k, target, s):
+        @pl.when(lax.rem(target, 2) == parity)
+        def _():
+            a_copy(1 + k, target, s, slab).wait_recv()
+            for i in range(1, nh):
+                @pl.when(target // 2 == lax.rem(chip + i, nh))
+                def _():
+                    add_pair(1 + k, target, s, slab)
+                    b_copy(1 + k, i, s, slab).start()
+
+    plans = (
+        [(1, 2, 0), (1, 3, 0), (1, 2, 1), (1, 3, 1), (0, 3, 1), (1, 0, 0), (1, 0, 1), (1, 1, 0), (1, 1, 1),
+         (0, 0, 0), (0, 0, 1), (0, 1, 0), (0, 1, 1)],
+        [(1, 0, 0), (1, 0, 1), (1, 1, 0), (1, 1, 1), (0, 1, 1), (1, 2, 0), (1, 3, 0), (1, 2, 1), (1, 3, 1),
+         (0, 2, 0), (0, 3, 0), (0, 2, 1), (0, 3, 1)],
+    )
+    near = chip == f // 2
+
+    def planned(n):
+        k, s, target = jnp.int32(0), jnp.int32(0), f
+        for plan, taken in zip(plans, (near, jnp.logical_not(near))):
+            for at, (kk, code, ss) in enumerate(plan):
+                here = jnp.logical_and(n == at, taken)
+                k = jnp.where(here, kk, k)
+                s = jnp.where(here, ss, s)
+                target = jnp.where(here, (f, mate, over, far)[code], target)
+        return k, target, s
+
+    def give_back(s):
+        for i in range(1, nh):
+            b_copy(2, i, s, slab).wait_recv()
+        for n in range(slab // LANES):
+            q = s * (slab // LANES) + n
+            back[pl.ds(q * LANES, LANES), :] = total_of(2, q).astype(BF)
+            g_copy(q).start()
+
+    def spread(q):
+        e_copy(q).wait_recv()
+        for i in range(1, nh):
+            c_copy(1, i, q).start()
+        d_copy(1, 0, q).start()
+
+    def hand_over(k, q):
+        for i in range(1, nh):
+            c_copy(k, i, q).wait_recv()
+            d_copy(k, i, q).start()
+
+    def second_norm(k):
+        for q in range(nq):
+            for i in range(nh):
+                d_copy(k, i, q).wait_recv()
+        normalize(functools.partial(chunk, x1.at[k]), g_ffn, put(h.at[k]), features // LANES)
+
+    @pl.when(inner)
+    def _():
+        cross(6, far)
+        hand_over(0, 0)
+        cross(7, over)
+        hand_over(0, 1)
+        spread(0)
+        cross(7, far)
+        hand_over(0, 2)
+        spread(1)
+        pass_on(8)
+        send_inner(9)
+        cross(8, over)
+        hand_over(0, 3)
+        spread(2)
+        second_norm(0)
+        cross(8, far)
+        spread(3)
+        settle(4)
+        settle(5)
+        project(0, 0)
+        pass_on(9)
+        hand_over(1, 0)
+        hand_over(1, 1)
+        settle(6)
+        settle(7)
+        project(0, 1)
+        cross(9, over)
+
+        @pl.when(near)
+        def _():
+            y_arrival(8, over)
+            mlp_out(0, over, 0)
+
+        @pl.when(jnp.logical_not(near))
+        def _():
+            mlp_out(0, f, 0)
+            mlp_out(0, f, 1)
+            pair_up(0, f, 0)
+
+        hand_over(1, 2)
+        hand_over(1, 3)
+        pair_up(0, jnp.where(near, over, f), jnp.where(near, 0, 1))
+        second_norm(1)
+        cross(9, far)
+
+        @pl.when(near)
+        def _():
+            y_arrival(8, far)
+
+        @pl.when(jnp.logical_not(near))
+        def _():
+            w_copy(8, mate).wait_recv()
+
+        ahead = jnp.where(near, far, mate)
+        mlp_out(0, ahead, 0)
+        project(1, 0)
+        pair_up(0, ahead, 0)
+
+        @pl.when(near)
+        def _():
+            y_arrival(9, over)
+            mlp_out(0, over, 1)
+
+        project(1, 1)
+
+        @pl.when(near)
+        def _():
+            pair_up(0, over, 1)
+
+
+        def ffn(n, carry):
+            near_waits = (
+                (3, lambda: y_arrival(9, far)),
+                (7, lambda: w_copy(8, mate).wait_recv()),
+                (8, lambda: w_copy(9, mate).wait_recv()),
+            )
+            away_waits = (
+                (3, lambda: w_copy(9, mate).wait_recv()),
+                (5, lambda: y_arrival(8, over)),
+                (6, lambda: y_arrival(8, far)),
+                (7, lambda: y_arrival(9, over)),
+                (8, lambda: y_arrival(9, far)),
+            )
+            for waits, taken in ((near_waits, near), (away_waits, jnp.logical_not(near))):
+                for at, wait in waits:
+                    @pl.when(jnp.logical_and(n == at, taken))
+                    def _():
+                        wait()
+
+            @pl.when(n == 10)
+            def _():
+                give_back(0)
+
+            mlp_out(*planned(n))
+
+            @pl.when(n >= 1)
+            def _():
+                pair_up(*planned(n - 1))
+            return carry
+
+        lax.fori_loop(0, len(plans[0]), ffn, 0)
+        pair_up(*planned(len(plans[0]) - 1))
+        give_back(1)
+        for q in range(nq):
+            for i in range(1, nh):
+                if q % (slab // LANES) == 0:
+                    b_copy(1, i, q // (slab // LANES), slab).wait_recv()
+            own_x[pl.ds(q * LANES, LANES), :] = x1[0, spot(t, q), :].astype(F32) + total_of(1, q)
+
+    @pl.when(outer)
+    def _():
+        for m in (8, 9):
+            w_copy(m, f).start()
+        for q in range(nq):
+            g_copy(q).wait_recv()
+            at = pl.ds(q * LANES, LANES)
+            own_x[at, :] = x1[0, spot(t, q), :].astype(F32) + home[at, :].astype(F32)
+
+    total = jnp.zeros((1, tokens), F32)
+    for q in range(nq):
+        v = own_x[pl.ds(q * LANES, LANES), :]
+        total += jnp.sum(v * v, axis=0, keepdims=True)
+    squares[0] = jnp.broadcast_to(total, squares.shape[1:])
+    for i in range(1, nt):
+        s_copy(i).start()
+
+    for i in range(1, nt):
+        s_copy(i).wait()
+    for i in range(1, nt):
+        total = total + squares[i, pl.ds(0, 1), :]
+    factor = lax.rsqrt(total / features + EPS)
+
+    def closing(q):
+        gain = column(g_out[pl.ds(t * nq + q, 1), :], tokens)
+        out[pl.ds(q * LANES, LANES), :] = (own_x[pl.ds(q * LANES, LANES), :] * factor * gain).astype(BF)
+
+    for q in range(nq):
+        closing(q)
+
+    for m in range(last):
+        in_copy(m, f, 0).wait_send()
+    for m in range(early):
+        for blk in blocks:
+            y_copy(m, blk, r).wait_send()
+    for i in range(1, nh + 1):
+        c = lax.rem(chip + i, nh)
+        a_copy(0, 2 * c + 1 - parity, 0, share).wait_send()
+    for i in range(1, nh):
+        for q in range(nq):
+            b_copy(0, i, q, LANES).wait_send()
+
+    @pl.when(inner)
+    def _():
+        for m in range(last):
+            in_copy(m, mate, 1).wait_send()
+        for m in range(early):
+            for j, blk in enumerate((f, over, far)):
+                out_copy(m, blk, j).wait_send()
+        for m in range(early, last):
+            if m != extra:
+                y_copy(m, over, r).wait_send()
+            y_copy(m, far, r).wait_send()
+        v_copy(f).wait_send()
+        for k in (0, 1):
+            for i in range(nh):
+                for s in range(cuts):
+                    a_copy(1 + k, 2 * i + 1 - parity, s, slab).wait_send()
+                    if i:
+                        b_copy(1 + k, i, s, slab).wait_send()
+                for q in range(nq):
+                    d_copy(k, i, q).wait_send()
+                    if i:
+                        c_copy(k, i, q).wait_send()
+        for q in range(nq):
+            g_copy(q).wait_send()
+
+    @pl.when(outer)
+    def _():
+        for m in range(early, last):
+            w_copy(m, f).wait_send()
+        for q in range(nq):
+            e_copy(q).wait_send()
+
+
 def solution(mesh):
     nr, nf, nt = mesh.shape["rep"], mesh.shape["fs"], mesh.shape["tp"]
+
+    def staged_call(act, w_in, w_out, w_gate, w_up, w_down, scale, g_mix, g_ffn, g_out):
+        features, tokens = act.shape
+        rows, channels = w_in.shape
+        ff = w_gate.shape[1]
+        share = features // nt
+        nh = nt // 2
+        nq = share // LANES
+        anywhere = pl.BlockSpec(memory_space=pl.ANY)
+        vmem = pl.BlockSpec(memory_space=pltpu.VMEM)
+        dma = pltpu.SemaphoreType.DMA
+        scratch = [
+            pltpu.VMEM((nf, rows, channels), BF),
+            pltpu.VMEM((nf, rows, channels), BF),
+            pltpu.VMEM((nf, ff, rows), BF),
+            pltpu.VMEM((nf, ff, rows), BF),
+            pltpu.VMEM((nf, ff, rows), BF),
+            pltpu.VMEM((features, tokens), BF),
+            pltpu.VMEM((2, features, tokens), BF),
+            pltpu.VMEM((2, features, tokens), BF),
+            pltpu.VMEM((3, features, tokens), BF),
+            pltpu.VMEM((channels, tokens), BF),
+            pltpu.VMEM((ff, tokens), F32),
+            pltpu.VMEM((ff, tokens), F32),
+            pltpu.VMEM((2, ff, tokens), BF),
+            pltpu.VMEM((share, tokens), F32),
+            pltpu.VMEM((nt, 8, tokens), F32),
+            pltpu.VMEM((3, nh, share, tokens), BF),
+            pltpu.VMEM((3, nh, share, tokens), BF),
+            pltpu.VMEM((share, tokens), BF),
+            pltpu.VMEM((share, tokens), BF),
+            dma((5,)), dma((4,)),
+            dma((10, 2)), dma((4, 3)), dma((10, nf)), dma((10,)), dma((10,)), dma((10, nf)), dma((10, nf)), dma((1,)), dma((1,)),
+            dma((3, nh, nq)), dma((3, nh, nq)), dma((3, nh, nq)), dma((3, nh, nq)),
+            dma((2, nh, nq)), dma((2, nh, nq)), dma((2, nh, nq)), dma((2, nh, nq)),
+            dma((nq,)), dma((nq,)), dma((nq,)), dma((nq,)), dma((nt,)), dma((nt,)),
+        ]
+        return pl.pallas_call(
+            functools.partial(staged, nr, nf, nt),
+            out_shape=jax.ShapeDtypeStruct((share, tokens), BF),
+            in_specs=[anywhere] * 6 + [vmem] * 4,
+            out_specs=vmem,
+            scratch_shapes=scratch,
+            compiler_params=pltpu.CompilerParams(
+                collective_id=0, has_side_effects=True, vmem_limit_bytes=60 * 1024 * 1024
+            ),
+        )(
+            act, w_in, w_out, w_gate.T, w_up.T, w_down.T,
+            *[v.reshape(-1, LANES) for v in (scale, g_mix, g_ffn, g_out)],
+        )
 
     def on_device(act, w_in, w_out, w_gate, w_up, w_down, scale, g_mix, g_ffn, g_out):
         features, tokens = act.shape
@@ -414,6 +1112,8 @@
         ff = w_gate.shape[1]
         share = features // nt
         nh = nt // 2
+        if nr == 2 and nf == 4 and share == rows and rows % (2 * nr * LANES) == 0 and ff % (32 * nr) == 0:
+            return staged_call(act, w_in, w_out, w_gate, w_up, w_down, scale, g_mix, g_ffn, g_out)
         anywhere = pl.BlockSpec(memory_space=pl.ANY)
         vmem = pl.BlockSpec(memory_space=pltpu.VMEM)
         dma = pltpu.SemaphoreType.DMA

time: 141 us -> 111 us (0.79)
  Pallas kernels: 133 us -> 109 us
  local copies, waits for them, and re-layouts: 7.67 us -> 1.87 us
    pallas_call x1, Pallas kernels: 133 us -> 109 us  [staged_call(): pl.pallas_call(functools.partial(staged, nr, nf, nt), out_shape=jax.Shape...]
    unnamed x6 -> x1, local copies, waits for them, and re-layouts: 7.67 us -> 1.87 us
where the time goes in v1:
time: 111 us
  Pallas kernels  109 us (98%)
  local copies, waits for them, and re-layouts  1.87 us (2%)
    pallas_call x1, Pallas kernels, staged_call(): pl.pallas_call(functools.partial(staged, nr, nf, nt), out_shape=jax.Shape...  109 us

profile of v1, /device:TPU:0, one launch (start us, length us, event | category | flops | bytes accessed | tf_op | source)
XLA Modules:
  0.0 110.8 jit_solution(16023592431804470996)
XLA Ops:
  0.0 108.9 %shard_map.100 = bf16[512,512]{1,0:T(8,128)(2,1)} custom-call(bf16[2048,512]{1,0:T(8,128)(2,1)} %act.1, bf16[512,256]{1,0:T(8,128)(2,1)} %w_in.1, bf16[512,256]{1,0:T(8,128)(2,1)} %w_out.1, bf16[704,512]{1,0:T(8,128)(2,1)} %bitcast.7, bf16[704,512]{1,0:T(8,128)(2,1)} %bitcast.8, bf16[704,512]{1,0:T(8,128)(2,1)} %bitcast.9, f32[8,128]{1,0:T(8,128)} %bitcast.13, ...), custom_call_target="tpu_custom_call" | custom-call | tf_op jit(solution)/shard_map/pallas_call | solution.py:1095
  108.9 1.9 %copy.12 = bf16[512,512]{1,0:T(8,128)(2,1)} copy(bf16[512,512]{1,0:T(8,128)(2,1)} %shard_map.100) | data formatting | bytes 1048576

commit v2 on v1

--- a/solution.py
+++ b/solution.py
@@ -409,9 +409,9 @@
     nr, nf, nt,
     act, w_in, w_out, w_gate, w_up, w_down, scale, g_mix, g_ffn, g_out, out,
     b_in, b_out, b_gate, b_up, b_down,
-    x0, h, x1, part, pooled, gate_acc, up_acc, hidden, own_x, squares,
+    x0, h, x1, part, pooled, gate_acc, up_acc, hidden, own_x, squares, power,
     buf_a, buf_b, back, home,
-    own_sem, act_sem, in_send, out_send, zrecv, wsend, wrecv, ysend, yrecv, v_send, v_recv,
+    own_sem, act_sem, in_send, out_send, zrecv, wrecv, ysend, yrecv, v_send, v_recv,
     a_send, a_recv, b_send, b_recv, c_send, c_recv, d_send, d_recv,
     e_send, e_recv, g_send, g_recv, s_send, s_recv,
 ):
@@ -443,11 +443,7 @@
     blocks = (mate, over, far)
 
     own = [pltpu.make_async_copy(shards[m], full[m].at[f], own_sem.at[m]) for m in range(5)]
-    quarter = features // 4
-    stream = [
-        pltpu.make_async_copy(act.at[pl.ds(i * quarter, quarter)], x0.at[pl.ds(i * quarter, quarter)], act_sem.at[i])
-        for i in range(4)
-    ]
+    stream = [pltpu.make_async_copy(act, x0, act_sem.at[0])]
     own[0].start()
     own[1].start()
     for copy in stream:
@@ -482,25 +478,40 @@
             src_ref=ref, dst_ref=dst, send_sem=send, recv_sem=recv, device_id=device, device_id_type=MESH
         )
 
+    def group(m):
+        return max(items[m][0] - 1, 0)
+
     def in_copy(m, blk, d):
         ref = part_of(m, blk, r)
-        return remote(ref, ref, in_send.at[m, d], zrecv.at[m, blk], (r, inward, t))
-
-    def out_copy(m, blk, d):
+        place = jnp.where(inner, 1, 0) if d == 0 else 2
+        return remote(ref, ref, in_send.at[group(m)], zrecv.at[m, place], (r, inward, t))
+
+    def out_copy(m, blk, j):
         ref = part_of(m, blk, r)
-        return remote(ref, ref, out_send.at[m, d], zrecv.at[m, blk], (r, mate, t))
+        return remote(ref, ref, out_send.at[0], zrecv.at[m, j], (r, mate, t))
+
+    def arrive(m, j):
+        ref = part_of(m, blocks[j], r)
+        remote(ref, ref, in_send.at[group(m)], zrecv.at[m, j], (r, mate, t)).wait_recv()
+
+    def lot(m):
+        return (m - early) // 2 if m < 2 * cuts + early else m - early - cuts
 
     def w_copy(m, blk):
         ref = part_of(m, blk, other_rep)
-        return remote(ref, ref, wsend.at[m], wrecv.at[m], (r, mate, t))
+        return remote(ref, ref, in_send.at[group(m)], wrecv.at[lot(m)], (r, mate, t))
 
     def v_copy(blk):
         ref = part_of(extra, blk, other_rep)
         return remote(ref, ref, v_send.at[0], v_recv.at[0], (r, inward, t))
 
-    def y_copy(m, blk, of):
-        ref = part_of(m, blk, of)
-        return remote(ref, ref, ysend.at[m, blk], yrecv.at[m, blk], (other_rep, f, t))
+    def y_copy(m, j, of):
+        ref = part_of(m, blocks[j], of)
+        place = m // 2 if m < last - 2 else last // 2 + 2 * (m - last + 2) + j - 2
+        return remote(ref, ref, ysend.at[group(m)], yrecv.at[place], (other_rep, f, t))
+
+    def y_lot(ref, place):
+        return remote(ref, ref, ysend.at[0], yrecv.at[place], (other_rep, f, t))
 
     def own_ready(m):
         if items[m][1] == 0:
@@ -515,30 +526,28 @@
             out_copy(m, f, 0).start()
 
     def hop(m, j):
-        blk = blocks[j]
-        in_copy(m, blk, 0).wait_recv()
+        arrive(m, j)
         if j == 0:
-            in_copy(m, blk, 1).start()
+            in_copy(m, mate, 1).start()
         else:
-            out_copy(m, blk, j).start()
+            out_copy(m, blocks[j], j).start()
 
     def side(m, j):
-        y_copy(m, blocks[j], r).start()
+        y_copy(m, j, r).start()
 
     def relay(m, j):
         hop(m, j)
         side(m, j)
 
     def collect(m, j):
-        in_copy(m, blocks[j], 0).wait_recv()
-        y_copy(m, blocks[j], r).start()
-
-    def y_arrival(m, blk):
-        y_copy(m, blk, other_rep).wait_recv()
-
-    def finish(m):
-        for blk in blocks:
-            y_arrival(m, blk)
+        arrive(m, j)
+        side(m, j)
+
+    def y_arrival(m, j):
+        y_copy(m, j, other_rep).wait_recv()
+
+    def finish(matrix):
+        y_lot(full[matrix].at[pl.ds(0, nf - 1), pl.ds(0, rows // nr)], matrix).wait_recv()
 
     def send_inner(m):
         in_copy(m, f, 0).start()
@@ -548,23 +557,21 @@
         w_copy(m, f).start()
 
     def pass_on(m):
-        if m < last:
-            in_copy(m, mate, 0).wait_recv()
-            in_copy(m, mate, 1).start()
+        hop(m, 0)
 
     def cross(m, *some):
-        for blk in some:
-            in_copy(m, blk, 0).wait_recv()
-            if m != extra or blk is far:
-                y_copy(m, blk, r).start()
-
-    def settle(m):
-        w_copy(m, mate).wait_recv()
-        if m == extra:
+        for j in some:
+            arrive(m, j)
+            if m != extra or j == 2:
+                side(m, j)
+
+    def settle(s):
+        ref = full[2].at[0, pl.ds(0, ff // cuts)]
+        remote(ref, ref, in_send.at[1], wrecv.at[s], (r, mate, t)).wait_recv()
+        pieces = 2 * nr - (s == cuts - 1)
+        y_lot(full[2].at[0, pl.ds(0, pieces * (ff // cuts // nr))], 2 + s).wait_recv()
+        if s == cuts - 1:
             v_copy(over).wait_recv()
-        else:
-            y_arrival(m, over)
-        y_arrival(m, far)
 
     def spot(target, q, size=LANES):
         return line(target * share + q * size, size)
@@ -594,33 +601,33 @@
     def a_copy(k, target, q, size):
         return remote(
             part.at[k, spot(target, q, size)], buf_a.at[k, target // 2, line(q * size, size)],
-            a_send.at[k, target // 2, q], a_recv.at[k, target // 2, q], (r, f, partner),
+            a_send.at[k], a_recv.at[k, target // 2, q], (r, f, partner),
         )
 
     def b_copy(k, i, q, size):
         target = 2 * lax.rem(chip + i, nh) + parity
         return remote(
             part.at[k, spot(target, q, size)], buf_b.at[k, i, line(q * size, size)],
-            b_send.at[k, i, q], b_recv.at[k, i, q], (r, f, target),
+            b_send.at[k], b_recv.at[k, i - 1, q], (r, f, target),
         )
 
     def c_copy(k, i, q):
         ref = x1.at[k, spot(t, q)]
         device = (r, f, 2 * lax.rem(chip + i, nh) + parity)
-        return remote(ref, ref, c_send.at[k, i, q], c_recv.at[k, i, q], device)
+        return remote(ref, ref, c_send.at[k], c_recv.at[k, i - 1, q], device)
 
     def d_copy(k, i, q):
         ref = x1.at[k, spot(2 * lax.rem(chip - i + nh, nh) + parity, q)]
-        return remote(ref, ref, d_send.at[k, i, q], d_recv.at[k, i, q], (r, f, partner))
+        return remote(ref, ref, d_send.at[k], d_recv.at[k, i], (r, f, partner))
 
     def e_copy(q):
-        return remote(x1.at[0, spot(t, q)], x1.at[1, spot(t, q)], e_send.at[q], e_recv.at[q], (r, mate, t))
+        return remote(x1.at[0, spot(t, q)], x1.at[1, spot(t, q)], e_send.at[0], e_recv.at[q], (r, mate, t))
 
     def g_copy(q):
-        return remote(back.at[line(q * LANES)], home.at[line(q * LANES)], g_send.at[q], g_recv.at[q], (r, mate, t))
+        return remote(back.at[line(q * LANES)], home.at[line(q * LANES)], g_send.at[0], g_recv.at[q], (r, mate, t))
 
     def s_copy(i):
-        return remote(squares.at[0], squares.at[i], s_send.at[i], s_recv.at[i], (r, f, lax.rem(t + i, nt)))
+        return remote(squares.at[0], squares.at[i], s_send.at[0], s_recv.at[0], (r, f, lax.rem(t + i, nt)))
 
     def add_pair(k, target, q, size):
         for n in range(size // LANES):
@@ -685,7 +692,6 @@
             collect(1, j)
 
     finish(0)
-    finish(1)
 
     u_mix = dot_first(b_in[0], h[0, pl.ds(0, rows), :])
     for b in range(1, nf):
@@ -715,10 +721,10 @@
     def _():
         relay(2, 2)
         relay(3, 2)
-        cross(4, over)
+        cross(4, 1)
         pass_on(5)
         send_inner(6)
-        cross(4, far)
+        cross(4, 2)
 
     @pl.when(outer)
     def _():
@@ -726,8 +732,7 @@
             collect(2, j)
             collect(3, j)
 
-    finish(2)
-    finish(3)
+    finish(1)
 
     def mix_out(target):
         part[0, line(target * share, share), :] = jnp.dot(
@@ -749,7 +754,15 @@
 
     @pl.when(inner)
     def _():
-        cross(5, over)
+        cross(5, 1)
+
+    def prepare(k, target, q):
+        at = spot(target, q)
+        v = x1[k, at, :].astype(F32)
+        h[k, at, :] = (v * column(g_ffn[pl.ds(target * nq + q, 1), :], tokens)).astype(BF)
+        power[k] += jnp.sum((v * v).reshape(LANES // 8, 8, tokens), axis=0)
+
+    power[...] = jnp.zeros_like(power)
 
     for q in range(nq):
         for i in range(1, nh):
@@ -761,51 +774,53 @@
             for i in range(1, nh):
                 c_copy(0, i, q).start()
             d_copy(0, 0, q).start()
+            prepare(0, t, q)
             if q == 0:
                 pass_on(6)
                 send_inner(7)
-                cross(5, far)
+                cross(5, 2)
             if q == 1:
-                cross(6, over)
+                cross(6, 1)
             if q == 2:
                 pass_on(7)
                 send_inner(8)
                 v_copy(f).start()
+                send_inner(9)
 
         @pl.when(outer)
         def _():
             e_copy(q).start()
-            if q == 0:
-                w_copy(7, f).start()
-            if q == 1:
-                in_copy(8, f, 0).start()
-            if q == 3:
-                in_copy(9, f, 0).start()
 
     cut = ff // cuts
     step = 32
     wide = 2 * LANES
 
-    def project(k, s):
+    def project(k, s, targets, fresh):
         at = pl.ds(s * cut, cut)
         for source, acc in ((b_gate, gate_acc), (b_up, up_acc)):
             def tokens_at(n, carry):
                 here = line(n * wide, wide)
-                total = jnp.dot(source[0, at, :], h[k, pl.ds(0, rows), here], preferred_element_type=F32)
-                for b in range(1, nf):
-                    total += jnp.dot(source[b, at, :], h[k, pl.ds(b * rows, rows), here], preferred_element_type=F32)
-                acc[at, here] = total
+                terms = [
+                    jnp.dot(source[b, at, :], h[k, line(b * rows, rows), here], preferred_element_type=F32)
+                    for b in targets
+                ]
+                total = functools.reduce(lambda x, y: x + y, terms)
+                acc[at, here] = total if fresh else acc[at, here] + total
                 return carry
 
             lax.fori_loop(0, tokens // wide, tokens_at, 0)
 
-        def activate(n, carry):
+    def activate(k, s):
+        total = jnp.sum(power[k], axis=0, keepdims=True)
+        factor = lax.rsqrt(total / features + EPS)
+
+        def some(n, carry):
             here = line(s * cut + n * step, step)
-            v = gate_acc[here, :]
-            hidden[k, here, :] = (v / (1.0 + jnp.exp(-v)) * up_acc[here, :]).astype(BF)
+            v = gate_acc[here, :] * factor
+            hidden[k, here, :] = (v / (1.0 + jnp.exp(-v)) * (up_acc[here, :] * factor)).astype(BF)
             return carry
 
-        lax.fori_loop(0, cut // step, activate, 0)
+        lax.fori_loop(0, cut // step, some, 0)
 
     def mlp_out(k, target, s):
         at = spot(target, s, slab)
@@ -826,10 +841,10 @@
                     b_copy(1 + k, i, s, slab).start()
 
     plans = (
-        [(1, 2, 0), (1, 3, 0), (1, 2, 1), (1, 3, 1), (0, 3, 1), (1, 0, 0), (1, 0, 1), (1, 1, 0), (1, 1, 1),
-         (0, 0, 0), (0, 0, 1), (0, 1, 0), (0, 1, 1)],
-        [(1, 0, 0), (1, 0, 1), (1, 1, 0), (1, 1, 1), (0, 1, 1), (1, 2, 0), (1, 3, 0), (1, 2, 1), (1, 3, 1),
-         (0, 2, 0), (0, 3, 0), (0, 2, 1), (0, 3, 1)],
+        [(1, 2, 0), (1, 3, 0), (1, 0, 0), (1, 1, 0), (1, 2, 1), (1, 3, 1), (1, 0, 1), (1, 1, 1),
+         (0, 2, 1), (0, 3, 0), (0, 3, 1), (0, 0, 0), (0, 0, 1), (0, 1, 0), (0, 1, 1)],
+        [(1, 0, 0), (1, 1, 0), (1, 2, 0), (1, 3, 0), (1, 0, 1), (1, 1, 1), (1, 2, 1), (1, 3, 1),
+         (0, 0, 1), (0, 1, 0), (0, 1, 1), (0, 2, 0), (0, 3, 0), (0, 2, 1), (0, 3, 1)],
     )
     near = chip == f // 2
 
@@ -856,101 +871,95 @@
         for i in range(1, nh):
             c_copy(1, i, q).start()
         d_copy(1, 0, q).start()
+        prepare(1, t, q)
+
+    def mine(i):
+        return 2 * lax.rem(chip - i + nh, nh) + parity
+
+    def theirs(i):
+        return 2 * lax.rem(chip - i + nh, nh) + 1 - parity
 
     def hand_over(k, q):
         for i in range(1, nh):
             c_copy(k, i, q).wait_recv()
             d_copy(k, i, q).start()
-
-    def second_norm(k):
+            prepare(k, mine(i), q)
+
+    def absorb(k, i):
+        ref = x1.at[k, line(theirs(i) * share, share)]
+        remote(ref, ref, d_send.at[k], d_recv.at[k, i], (r, f, partner)).wait_recv()
         for q in range(nq):
-            for i in range(nh):
-                d_copy(k, i, q).wait_recv()
-        normalize(functools.partial(chunk, x1.at[k]), g_ffn, put(h.at[k]), features // LANES)
+            prepare(k, theirs(i), q)
+
+    here_blocks = (t, partner)
+    away_blocks = tuple(b for i in range(1, nh) for b in (mine(i), theirs(i)))
 
     @pl.when(inner)
     def _():
-        cross(6, far)
+        cross(6, 2)
+        absorb(0, 0)
         hand_over(0, 0)
-        cross(7, over)
+        cross(7, 1)
         hand_over(0, 1)
         spread(0)
-        cross(7, far)
+        cross(7, 2)
         hand_over(0, 2)
         spread(1)
-        pass_on(8)
-        send_inner(9)
-        cross(8, over)
+        cross(8, 1)
         hand_over(0, 3)
         spread(2)
-        second_norm(0)
-        cross(8, far)
         spread(3)
-        settle(4)
-        settle(5)
-        project(0, 0)
-        pass_on(9)
+        for i in range(1, nh):
+            absorb(0, i)
+        settle(0)
+        project(0, 0, here_blocks + away_blocks, True)
+        activate(0, 0)
         hand_over(1, 0)
+        settle(1)
+        project(0, 1, here_blocks + away_blocks, True)
+        activate(0, 1)
+        pass_on(8)
         hand_over(1, 1)
-        settle(6)
-        settle(7)
-        project(0, 1)
-        cross(9, over)
 
         @pl.when(near)
         def _():
-            y_arrival(8, over)
-            mlp_out(0, over, 0)
-
-        @pl.when(jnp.logical_not(near))
-        def _():
-            mlp_out(0, f, 0)
-            mlp_out(0, f, 1)
-            pair_up(0, f, 0)
-
+            y_arrival(8, 1)
+
+        lead = jnp.where(near, over, f)
+        mlp_out(0, lead, 0)
+
+        absorb(1, 0)
+        project(1, 0, here_blocks, True)
         hand_over(1, 2)
+        cross(9, 1)
+        pair_up(0, lead, 0)
+        pass_on(9)
+        project(1, 1, here_blocks, True)
+        cross(8, 2)
         hand_over(1, 3)
-        pair_up(0, jnp.where(near, over, f), jnp.where(near, 0, 1))
-        second_norm(1)
-        cross(9, far)
-
-        @pl.when(near)
-        def _():
-            y_arrival(8, far)
-
-        @pl.when(jnp.logical_not(near))
-        def _():
-            w_copy(8, mate).wait_recv()
-
-        ahead = jnp.where(near, far, mate)
-        mlp_out(0, ahead, 0)
-        project(1, 0)
-        pair_up(0, ahead, 0)
-
-        @pl.when(near)
-        def _():
-            y_arrival(9, over)
-            mlp_out(0, over, 1)
-
-        project(1, 1)
-
-        @pl.when(near)
-        def _():
-            pair_up(0, over, 1)
-
+        for i in range(1, nh):
+            absorb(1, i)
+        project(1, 0, away_blocks, False)
+        activate(1, 0)
+        project(1, 1, away_blocks, False)
+        activate(1, 1)
+        cross(9, 2)
 
         def ffn(n, carry):
             near_waits = (
-                (3, lambda: y_arrival(9, far)),
-                (7, lambda: w_copy(8, mate).wait_recv()),
-                (8, lambda: w_copy(9, mate).wait_recv()),
+                (1, lambda: y_arrival(8, 2)),
+                (3, lambda: w_copy(8, mate).wait_recv()),
+                (4, lambda: y_arrival(9, 1)),
+                (5, lambda: y_arrival(9, 2)),
+                (7, lambda: w_copy(9, mate).wait_recv()),
             )
             away_waits = (
-                (3, lambda: w_copy(9, mate).wait_recv()),
-                (5, lambda: y_arrival(8, over)),
-                (6, lambda: y_arrival(8, far)),
-                (7, lambda: y_arrival(9, over)),
-                (8, lambda: y_arrival(9, far)),
+                (1, lambda: w_copy(8, mate).wait_recv()),
+                (2, lambda: y_arrival(8, 1)),
+                (3, lambda: y_arrival(8, 2)),
+                (5, lambda: w_copy(9, mate).wait_recv()),
+                (6, lambda: y_arrival(9, 1)),
+                (7, lambda: y_arrival(9, 2)),
             )
             for waits, taken in ((near_waits, near), (away_waits, jnp.logical_not(near))):
                 for at, wait in waits:
@@ -980,6 +989,9 @@
 
     @pl.when(outer)
     def _():
+        w_copy(7, f).start()
+        for m in (8, 9):
+            in_copy(m, f, 0).start()
         for m in (8, 9):
             w_copy(m, f).start()
         for q in range(nq):
@@ -995,8 +1007,8 @@
     for i in range(1, nt):
         s_copy(i).start()
 
-    for i in range(1, nt):
-        s_copy(i).wait()
+    got = squares.at[pl.ds(1, nt - 1)]
+    remote(got, got, s_send.at[0], s_recv.at[0], (r, f, partner)).wait_recv()
     for i in range(1, nt):
         total = total + squares[i, pl.ds(0, 1), :]
     factor = lax.rsqrt(total / features + EPS)
@@ -1008,49 +1020,35 @@
     for q in range(nq):
         closing(q)
 
-    for m in range(last):
-        in_copy(m, f, 0).wait_send()
-    for m in range(early):
-        for blk in blocks:
-            y_copy(m, blk, r).wait_send()
-    for i in range(1, nh + 1):
-        c = lax.rem(chip + i, nh)
-        a_copy(0, 2 * c + 1 - parity, 0, share).wait_send()
-    for i in range(1, nh):
-        for q in range(nq):
-            b_copy(0, i, q, LANES).wait_send()
+    def sent(ref, sem):
+        remote(ref, ref, sem, zrecv.at[0, 0], (r, mate, t)).wait_send()
+
+    for matrix in (2, 3, 4):
+        sent(full[matrix].at[0], in_send.at[matrix - 1])
+    sent(full[0].at[pl.ds(0, nf - 1)], ysend.at[0])
+    sent(part.at[0, pl.ds(0, nh * share)], a_send.at[0])
+    sent(part.at[0, pl.ds(0, (nh - 1) * share)], b_send.at[0])
+    sent(squares.at[pl.ds(1, nt - 1)], s_send.at[0])
 
     @pl.when(inner)
     def _():
-        for m in range(last):
-            in_copy(m, mate, 1).wait_send()
-        for m in range(early):
-            for j, blk in enumerate((f, over, far)):
-                out_copy(m, blk, j).wait_send()
-        for m in range(early, last):
-            if m != extra:
-                y_copy(m, over, r).wait_send()
-            y_copy(m, far, r).wait_send()
+        sent(full[0].at[pl.ds(0, 2)], in_send.at[0])
+        sent(full[0].at[pl.ds(0, nf - 1)], out_send.at[0])
         v_copy(f).wait_send()
+        sent(full[2].at[0], ysend.at[1])
+        sent(full[3].at[0, pl.ds(0, (2 * nr - 1) * (ff // cuts // nr))], ysend.at[2])
+        sent(full[4].at[0], ysend.at[3])
         for k in (0, 1):
-            for i in range(nh):
-                for s in range(cuts):
-                    a_copy(1 + k, 2 * i + 1 - parity, s, slab).wait_send()
-                    if i:
-                        b_copy(1 + k, i, s, slab).wait_send()
-                for q in range(nq):
-                    d_copy(k, i, q).wait_send()
-                    if i:
-                        c_copy(k, i, q).wait_send()
-        for q in range(nq):
-            g_copy(q).wait_send()
+            sent(part.at[0, pl.ds(0, nh * share)], a_send.at[1 + k])
+            sent(part.at[0, pl.ds(0, (nh - 1) * share)], b_send.at[1 + k])
+            sent(part.at[0, pl.ds(0, nh * share)], d_send.at[k])
+            sent(part.at[0, pl.ds(0, (nh - 1) * share)], c_send.at[k])
+        sent(back, g_send.at[0])
 
     @pl.when(outer)
     def _():
-        for m in range(early, last):
-            w_copy(m, f).wait_send()
-        for q in range(nq):
-            e_copy(q).wait_send()
+        sent(full[0].at[0], in_send.at[0])
+        sent(back, e_send.at[0])
 
 
 def solution(mesh):
@@ -1082,15 +1080,16 @@
             pltpu.VMEM((2, ff, tokens), BF),
             pltpu.VMEM((share, tokens), F32),
             pltpu.VMEM((nt, 8, tokens), F32),
+            pltpu.VMEM((2, 8, tokens), F32),
             pltpu.VMEM((3, nh, share, tokens), BF),
             pltpu.VMEM((3, nh, share, tokens), BF),
             pltpu.VMEM((share, tokens), BF),
             pltpu.VMEM((share, tokens), BF),
-            dma((5,)), dma((4,)),
-            dma((10, 2)), dma((4, 3)), dma((10, nf)), dma((10,)), dma((10,)), dma((10, nf)), dma((10, nf)), dma((1,)), dma((1,)),
-            dma((3, nh, nq)), dma((3, nh, nq)), dma((3, nh, nq)), dma((3, nh, nq)),
-            dma((2, nh, nq)), dma((2, nh, nq)), dma((2, nh, nq)), dma((2, nh, nq)),
-            dma((nq,)), dma((nq,)), dma((nq,)), dma((nq,)), dma((nt,)), dma((nt,)),
+            dma((5,)), dma((1,)),
+            dma((4,)), dma((1,)), dma((10, 3)), dma((4,)), dma((4,)), dma((8,)), dma((1,)), dma((1,)),
+            dma((3,)), dma((3, nh, 2)), dma((3,)), dma((3, nh - 1, nq)),
+            dma((2,)), dma((2, nh - 1, nq)), dma((2,)), dma((2, nh)),
+            dma((1,)), dma((nq,)), dma((1,)), dma((nq,)), dma((1,)), dma((1,)),
         ]
         return pl.pallas_call(
             functools.partial(staged, nr, nf, nt),

time: 111 us -> 102 us (0.919)
  Pallas kernels: 109 us -> 100 us
    pallas_call x1, Pallas kernels: 109 us -> 100 us  [staged_call(): pl.pallas_call(functools.partial(staged, nr, nf, nt), out_shape=jax.Shape...]
where the time goes in v2:
time: 102 us
  Pallas kernels  100 us (98%)
  local copies, waits for them, and re-layouts  1.87 us (2%)
    pallas_call x1, Pallas kernels, staged_call(): pl.pallas_call(functools.partial(staged, nr, nf, nt), out_shape=jax.Shape...  100 us

profile of v2, /device:TPU:0, one launch (start us, length us, event | category | flops | bytes accessed | tf_op | source)
XLA Modules:
  0.0 102.0 jit_solution(14194782398953875718)
XLA Ops:
  0.0 100.1 %shard_map.100 = bf16[512,512]{1,0:T(8,128)(2,1)} custom-call(bf16[2048,512]{1,0:T(8,128)(2,1)} %act.1, bf16[512,256]{1,0:T(8,128)(2,1)} %w_in.1, bf16[512,256]{1,0:T(8,128)(2,1)} %w_out.1, bf16[704,512]{1,0:T(8,128)(2,1)} %bitcast.7, bf16[704,512]{1,0:T(8,128)(2,1)} %bitcast.8, bf16[704,512]{1,0:T(8,128)(2,1)} %bitcast.9, f32[8,128]{1,0:T(8,128)} %bitcast.13, ...), custom_call_target="tpu_custom_call" | custom-call | tf_op jit(solution)/shard_map/pallas_call | solution.py:1094
  100.1 1.9 %copy.12 = bf16[512,512]{1,0:T(8,128)(2,1)} copy(bf16[512,512]{1,0:T(8,128)(2,1)} %shard_map.100) | data formatting | bytes 1048576

commit v3 on v2

--- a/solution.py
+++ b/solution.py
@@ -508,6 +508,8 @@
     def y_copy(m, j, of):
         ref = part_of(m, blocks[j], of)
         place = m // 2 if m < last - 2 else last // 2 + 2 * (m - last + 2) + j - 2
+        if items[m][0] == 1 and j == 0:
+            place = last - 2
         return remote(ref, ref, ysend.at[group(m)], yrecv.at[place], (other_rep, f, t))
 
     def y_lot(ref, place):
@@ -546,8 +548,8 @@
     def y_arrival(m, j):
         y_copy(m, j, other_rep).wait_recv()
 
-    def finish(matrix):
-        y_lot(full[matrix].at[pl.ds(0, nf - 1), pl.ds(0, rows // nr)], matrix).wait_recv()
+    def finish(matrix, count, place):
+        y_lot(full[matrix].at[pl.ds(0, count), pl.ds(0, rows // nr)], place).wait_recv()
 
     def send_inner(m):
         in_copy(m, f, 0).start()
@@ -654,7 +656,7 @@
             in_copy(m, f, 0).start()
         for m in (4, 5, 6):
             send_outer(m)
-        in_copy(7, f, 0).start()
+        send_outer(7)
 
     @pl.when(inner)
     def _():
@@ -674,12 +676,8 @@
         hop(2, 0)
         hop(3, 0)
         send_inner(4)
-        for m in (2, 3):
-            out_copy(m, f, 0).start()
         relay(0, 2)
         relay(1, 2)
-        side(2, 0)
-        side(3, 0)
         relay(2, 1)
         relay(3, 1)
         pass_on(4)
@@ -691,7 +689,7 @@
             collect(0, j)
             collect(1, j)
 
-    finish(0)
+    finish(0, nf - 1, 0)
 
     u_mix = dot_first(b_in[0], h[0, pl.ds(0, rows), :])
     for b in range(1, nf):
@@ -717,40 +715,66 @@
 
     mixed = True
 
-    @pl.when(inner)
-    def _():
-        relay(2, 2)
-        relay(3, 2)
-        cross(4, 1)
-        pass_on(5)
-        send_inner(6)
-        cross(4, 2)
-
-    @pl.when(outer)
-    def _():
-        for j in range(3):
-            collect(2, j)
-            collect(3, j)
-
-    finish(1)
-
     def mix_out(target):
         part[0, line(target * share, share), :] = jnp.dot(
             b_out[target], pooled[...], preferred_element_type=F32
         ).astype(BF)
 
-    for i in range(1, nh + 1):
-        c = lax.rem(chip + i, nh)
-        mix_out(2 * c + 1 - parity)
-        a_copy(0, 2 * c + 1 - parity, 0, share).start()
-        mix_out(2 * c + parity)
-    for i in range(1, nh):
-        target = 2 * lax.rem(chip + i, nh) + parity
-        a_copy(0, target, 0, share).wait_recv()
-        for q in range(nq):
-            add_pair(0, target, q, LANES)
-            b_copy(0, i, q, LANES).start()
-    a_copy(0, t, 0, share).wait_recv()
+        @pl.when(lax.rem(target, 2) != parity)
+        def _():
+            a_copy(0, target, 0, share).start()
+
+    def reduce_pair(target):
+        @pl.when(lax.rem(target, 2) == parity)
+        def _():
+            a_copy(0, target, 0, share).wait_recv()
+            for i in range(1, nh):
+                @pl.when(target // 2 == lax.rem(chip + i, nh))
+                def _():
+                    for q in range(nq):
+                        add_pair(0, target, q, LANES)
+                        b_copy(0, i, q, LANES).start()
+
+    mix_out(f)
+
+    @pl.when(inner)
+    def _():
+        relay(2, 2)
+        relay(3, 2)
+        side(2, 0)
+        side(3, 0)
+        for m in (2, 3):
+            out_copy(m, f, 0).start()
+
+    reduce_pair(f)
+
+    @pl.when(inner)
+    def _():
+        cross(4, 1)
+        pass_on(5)
+        send_inner(6)
+
+    @pl.when(outer)
+    def _():
+        for j in (1, 2):
+            collect(2, j)
+            collect(3, j)
+        collect(2, 0)
+        collect(3, 0)
+
+    finish(1, 2, 1)
+    mix_out(over)
+    mix_out(far)
+    reduce_pair(over)
+    reduce_pair(far)
+
+    @pl.when(inner)
+    def _():
+        cross(4, 2)
+
+    finish(1, 1, last - 2)
+    mix_out(mate)
+    reduce_pair(mate)
 
     @pl.when(inner)
     def _():
@@ -783,8 +807,8 @@
                 cross(6, 1)
             if q == 2:
                 pass_on(7)
+                v_copy(f).start()
                 send_inner(8)
-                v_copy(f).start()
                 send_inner(9)
 
         @pl.when(outer)
@@ -841,11 +865,12 @@
                     b_copy(1 + k, i, s, slab).start()
 
     plans = (
-        [(1, 2, 0), (1, 3, 0), (1, 0, 0), (1, 1, 0), (1, 2, 1), (1, 3, 1), (1, 0, 1), (1, 1, 1),
+        [(1, 2, 0), (1, 2, 1), (1, 0, 0), (1, 0, 1), (1, 3, 0), (1, 1, 0), (1, 3, 1), (1, 1, 1),
          (0, 2, 1), (0, 3, 0), (0, 3, 1), (0, 0, 0), (0, 0, 1), (0, 1, 0), (0, 1, 1)],
-        [(1, 0, 0), (1, 1, 0), (1, 2, 0), (1, 3, 0), (1, 0, 1), (1, 1, 1), (1, 2, 1), (1, 3, 1),
+        [(1, 0, 0), (1, 0, 1), (1, 1, 0), (1, 2, 0), (1, 2, 1), (1, 1, 1), (1, 3, 0), (1, 3, 1),
          (0, 0, 1), (0, 1, 0), (0, 1, 1), (0, 2, 0), (0, 3, 0), (0, 2, 1), (0, 3, 1)],
     )
+    soon = jnp.logical_or(t == f, t == over)
     near = chip == f // 2
 
     def planned(n):
@@ -899,27 +924,34 @@
         cross(6, 2)
         absorb(0, 0)
         hand_over(0, 0)
+        settle(0)
+        project(0, 0, here_blocks, True)
         cross(7, 1)
         hand_over(0, 1)
         spread(0)
         cross(7, 2)
         hand_over(0, 2)
         spread(1)
-        cross(8, 1)
         hand_over(0, 3)
         spread(2)
-        spread(3)
         for i in range(1, nh):
             absorb(0, i)
-        settle(0)
-        project(0, 0, here_blocks + away_blocks, True)
+        project(0, 0, away_blocks, False)
         activate(0, 0)
+        spread(3)
         hand_over(1, 0)
+        absorb(1, 0)
+        project(1, 0, here_blocks, True)
+        cross(8, 1)
+        pass_on(8)
+        hand_over(1, 1)
         settle(1)
         project(0, 1, here_blocks + away_blocks, True)
         activate(0, 1)
-        pass_on(8)
-        hand_over(1, 1)
+        hand_over(1, 2)
+        pass_on(9)
+        project(1, 1, here_blocks, True)
+        cross(9, 1)
 
         @pl.when(near)
         def _():
@@ -927,38 +959,31 @@
 
         lead = jnp.where(near, over, f)
         mlp_out(0, lead, 0)
-
-        absorb(1, 0)
-        project(1, 0, here_blocks, True)
-        hand_over(1, 2)
-        cross(9, 1)
-        pair_up(0, lead, 0)
-        pass_on(9)
-        project(1, 1, here_blocks, True)
-        cross(8, 2)
         hand_over(1, 3)
         for i in range(1, nh):
             absorb(1, i)
+        cross(8, 2)
+        pair_up(0, lead, 0)
         project(1, 0, away_blocks, False)
         activate(1, 0)
         project(1, 1, away_blocks, False)
+        cross(9, 2)
         activate(1, 1)
-        cross(9, 2)
 
         def ffn(n, carry):
             near_waits = (
-                (1, lambda: y_arrival(8, 2)),
-                (3, lambda: w_copy(8, mate).wait_recv()),
-                (4, lambda: y_arrival(9, 1)),
-                (5, lambda: y_arrival(9, 2)),
+                (1, lambda: y_arrival(9, 1)),
+                (4, lambda: y_arrival(8, 2)),
+                (5, lambda: w_copy(8, mate).wait_recv()),
+                (6, lambda: y_arrival(9, 2)),
                 (7, lambda: w_copy(9, mate).wait_recv()),
             )
             away_waits = (
-                (1, lambda: w_copy(8, mate).wait_recv()),
-                (2, lambda: y_arrival(8, 1)),
-                (3, lambda: y_arrival(8, 2)),
+                (2, lambda: w_copy(8, mate).wait_recv()),
+                (3, lambda: y_arrival(8, 1)),
+                (4, lambda: y_arrival(9, 1)),
                 (5, lambda: w_copy(9, mate).wait_recv()),
-                (6, lambda: y_arrival(9, 1)),
+                (6, lambda: y_arrival(8, 2)),
                 (7, lambda: y_arrival(9, 2)),
             )
             for waits, taken in ((near_waits, near), (away_waits, jnp.logical_not(near))):
@@ -967,9 +992,10 @@
                     def _():
                         wait()
 
-            @pl.when(n == 10)
-            def _():
-                give_back(0)
+            for s, first, second in ((0, 8, 10), (1, 9, 13)):
+                @pl.when(n == jnp.where(soon, first, second))
+                def _():
+                    give_back(s)
 
             mlp_out(*planned(n))
 
@@ -980,7 +1006,6 @@
 
         lax.fori_loop(0, len(plans[0]), ffn, 0)
         pair_up(*planned(len(plans[0]) - 1))
-        give_back(1)
         for q in range(nq):
             for i in range(1, nh):
                 if q % (slab // LANES) == 0:
@@ -989,7 +1014,6 @@
 
     @pl.when(outer)
     def _():
-        w_copy(7, f).start()
         for m in (8, 9):
             in_copy(m, f, 0).start()
         for m in (8, 9):
@@ -1086,7 +1110,7 @@
             pltpu.VMEM((share, tokens), BF),
             pltpu.VMEM((share, tokens), BF),
             dma((5,)), dma((1,)),
-            dma((4,)), dma((1,)), dma((10, 3)), dma((4,)), dma((4,)), dma((8,)), dma((1,)), dma((1,)),
+            dma((4,)), dma((1,)), dma((10, 3)), dma((4,)), dma((4,)), dma((9,)), dma((1,)), dma((1,)),
             dma((3,)), dma((3, nh, 2)), dma((3,)), dma((3, nh - 1, nq)),
             dma((2,)), dma((2, nh - 1, nq)), dma((2,)), dma((2, nh)),
             dma((1,)), dma((nq,)), dma((1,)), dma((nq,)), dma((1,)), dma((1,)),

time: 102 us -> 99.7 us (0.977)
  Pallas kernels: 100 us -> 97.6 us
    pallas_call x1, Pallas kernels: 100 us -> 97.6 us  [staged_call(): pl.pallas_call(functools.partial(staged, nr, nf, nt), out_shape=jax.Shape...]
where the time goes in v3:
time: 99.7 us; the launch traced here: 99.5 us
  Pallas kernels  97.6 us (98%)
  local copies, waits for them, and re-layouts  1.87 us (2%)
    pallas_call x1, Pallas kernels, staged_call(): pl.pallas_call(functools.partial(staged, nr, nf, nt), out_shape=jax.Shape...  97.6 us

profile of v3, /device:TPU:0, one launch (start us, length us, event | category | flops | bytes accessed | tf_op | source)
XLA Modules:
  0.0 99.5 jit_solution(16148457668377781537)
XLA Ops:
  0.0 97.6 %shard_map.100 = bf16[512,512]{1,0:T(8,128)(2,1)} custom-call(bf16[2048,512]{1,0:T(8,128)(2,1)} %act.1, bf16[512,256]{1,0:T(8,128)(2,1)} %w_in.1, bf16[512,256]{1,0:T(8,128)(2,1)} %w_out.1, bf16[704,512]{1,0:T(8,128)(2,1)} %bitcast.7, bf16[704,512]{1,0:T(8,128)(2,1)} %bitcast.8, bf16[704,512]{1,0:T(8,128)(2,1)} %bitcast.9, f32[8,128]{1,0:T(8,128)} %bitcast.13, ...), custom_call_target="tpu_custom_call" | custom-call | tf_op jit(solution)/shard_map/pallas_call | solution.py:1118
  97.6 1.9 %copy.12 = bf16[512,512]{1,0:T(8,128)(2,1)} copy(bf16[512,512]{1,0:T(8,128)(2,1)} %shard_map.100) | data formatting | bytes 1048576

commit v4 on v3

--- a/solution.py
+++ b/solution.py
@@ -992,16 +992,17 @@
                     def _():
                         wait()
 
+            mlp_out(*planned(n))
+
+            @pl.when(n >= 1)
+            def _():
+                pair_up(*planned(n - 1))
+
             for s, first, second in ((0, 8, 10), (1, 9, 13)):
                 @pl.when(n == jnp.where(soon, first, second))
                 def _():
                     give_back(s)
 
-            mlp_out(*planned(n))
-
-            @pl.when(n >= 1)
-            def _():
-                pair_up(*planned(n - 1))
             return carry
 
         lax.fori_loop(0, len(plans[0]), ffn, 0)

time: 99.7 us -> 99.6 us (level)
  no operation moved by 1% of the time
where the time goes in v4:
time: 99.6 us; the launch traced here: 99.4 us
  Pallas kernels  97.5 us (98%)
  local copies, waits for them, and re-layouts  1.87 us (2%)
    pallas_call x1, Pallas kernels, staged_call(): pl.pallas_call(functools.partial(staged, nr, nf, nt), out_shape=jax.Shape...  97.5 us

profile of v4, /device:TPU:0, one launch (start us, length us, event | category | flops | bytes accessed | tf_op | source)
XLA Modules:
  0.0 99.4 jit_solution(2949538958103811716)
XLA Ops:
  0.0 97.5 %shard_map.100 = bf16[512,512]{1,0:T(8,128)(2,1)} custom-call(bf16[2048,512]{1,0:T(8,128)(2,1)} %act.1, bf16[512,256]{1,0:T(8,128)(2,1)} %w_in.1, bf16[512,256]{1,0:T(8,128)(2,1)} %w_out.1, bf16[704,512]{1,0:T(8,128)(2,1)} %bitcast.7, bf16[704,512]{1,0:T(8,128)(2,1)} %bitcast.8, bf16[704,512]{1,0:T(8,128)(2,1)} %bitcast.9, f32[8,128]{1,0:T(8,128)} %bitcast.13, ...), custom_call_target="tpu_custom_call" | custom-call | tf_op jit(solution)/shard_map/pallas_call | solution.py:1119
  97.5 1.9 %copy.12 = bf16[512,512]{1,0:T(8,128)(2,1)} copy(bf16[512,512]{1,0:T(8,128)(2,1)} %shard_map.100) | data formatting | bytes 1048576
